TPU v7x, 32 devices: a whole 2x2x4 slice. The times are simulated.
32 devices in a mesh: grp: 2 (over y), ep: 4 (over z), tp: 4 (over x, core).
Axes of the slice: x: 2, y: 2, z: 4, core: 2. Of those that a mesh axis runs over, the one named last changes fastest.
Arguments:
- query_plain: bfloat16 [2048, 512], P(('grp', 'ep'), 'tp'), parts along dimension 0, may hold values from -400 to 400
- query_rotary: bfloat16 [2048, 256], P(('grp', 'ep'), 'tp'), parts along dimension 0, may hold values from -6 to 6
- latent_input: bfloat16 [2048, 256], P(('grp', 'ep')), parts along dimension 0, may hold values from -6 to 6
- rotary_key: bfloat16 [2048, 32], P(('grp', 'ep')), parts along dimension 0, may hold values from -6 to 6
- key_weight: bfloat16 [256, 512], P(None, 'tp'), may hold values from -0.375 to 0.375
- value_weight: bfloat16 [256, 512], P(None, 'tp'), may hold values from -0.375 to 0.375
- latent_gain: bfloat16 [256], replicated, may hold values from 0.099609375 to 1.8984375
- head_gain: bfloat16 [512], P('tp'), may hold values from 0.099609375 to 1.8984375
- out_weight: bfloat16 [512, 2048], P('tp'), may hold values from -0.25 to 0.25
- expert_input: bfloat16 [4096, 2048], P(('grp', 'ep', 'tp')), parts along dimension 0, may hold values from -6 to 6
- expert_gain: bfloat16 [2048], replicated, may hold values from 0.099609375 to 1.8984375
- routes: int32 [4096, 2], P(('grp', 'ep', 'tp')), parts along dimension 0, may hold values from 0 to 3, all different within a row; in each aligned block of 128 rows (0 to 127, 128 to 255, ...) at most 72 rows name the same one
- route_weight: float32 [4096, 2], P(('grp', 'ep', 'tp')), parts along dimension 0, may hold values from 0.1 to 1
- gate_weight: bfloat16 [4, 2048, 3584], P('ep', None, 'tp'), may hold values from -0.125 to 0.125
- up_weight: bfloat16 [4, 2048, 3584], P('ep', None, 'tp'), may hold values from -0.125 to 0.125
- down_weight: bfloat16 [4, 3584, 2048], P('ep', 'tp'), may hold values from -0.09375 to 0.09375
Outputs:
- attended: bfloat16 [2048, 2048], P(('grp', 'ep', 'tp')), parts along dimension 0
- expert_out: bfloat16 [4096, 2048], P(('grp', 'ep', 'tp')), parts along dimension 0
There are 2 independent parts, one for each index of `grp`. A program takes and returns all parts, laid end to end along the dimension named above; an argument that names none is the same for every part. Nothing has to cross between parts.
Inputs may be any that keep to these rules, and one draw needn't show every extreme that they name: `routes`: each of the 128 rows of one device names 2 different experts; no expert is named by more than 72 rows of one device, a bound that some block reaches of some device.
All inputs are finite; a program needn't handle non-finite values.
Results may differ from a plain program's by a relative error of at most 0.012.
Values may be sent and summed in bfloat16 or wider, within the bound.
A program may use at most 128 MiB of HBM per device.

v0:
```python
import jax
import jax.numpy as jnp
from jax import lax
from jax.sharding import PartitionSpec as P

PLAIN_DIM = 64
ROTARY_DIM = 32
VALUE_DIM = 64
TOP = 2


EPSILON = 1e-06
THETA = 10000.0
key_span = 2048


def normalize(entries, gain):
    wide = entries.astype(jnp.float32)
    factor = lax.rsqrt(jnp.mean(wide * wide, axis=-1, keepdims=True) + EPSILON)
    return wide * factor * gain.astype(jnp.float32)


def rotate(entries, positions):
    half = entries.shape[-1] // 2
    freqs = THETA ** (-jnp.arange(half, dtype=jnp.float32) / half)
    angle = positions.astype(jnp.float32)[:, None, None] * freqs[None, None, :]
    cosine = jnp.cos(angle)
    sine = jnp.sin(angle)
    first = entries[..., :half].astype(jnp.float32)
    second = entries[..., half:].astype(jnp.float32)
    turned = jnp.concatenate(
        [first * cosine - second * sine, first * sine + second * cosine], axis=-1
    )
    return turned.astype(jnp.bfloat16)


def rounded(entries):
    return lax.optimization_barrier(entries.astype(jnp.bfloat16)).astype(jnp.float32)


def attend(
    query_plain,
    query_rotary,
    latent_input,
    rotary_key,
    key_weight,
    value_weight,
    latent_gain,
    head_gain,
    out_weight,
):
    tokens = query_plain.shape[0]
    heads = key_weight.shape[1] // PLAIN_DIM
    offset = lax.axis_index("ep") * tokens
    positions = offset + jnp.arange(tokens, dtype=jnp.int32)
    last_position = offset + tokens - 1
    latent = normalize(latent_input, latent_gain).astype(jnp.bfloat16)
    key_rotated = rotate(rotary_key.reshape(tokens, 1, ROTARY_DIM), positions).reshape(
        tokens, ROTARY_DIM
    )
    query_rotated = rotate(query_rotary.reshape(tokens, heads, ROTARY_DIM), positions)
    queries = query_plain.reshape(tokens, heads, PLAIN_DIM)
    factor = (PLAIN_DIM + ROTARY_DIM) ** (-0.5)

    def expand_latent(piece):
        latent_rows, key_rows = piece
        count = latent_rows.shape[0]
        keys = jnp.dot(latent_rows, key_weight, preferred_element_type=jnp.float32).astype(
            jnp.bfloat16
        )
        values = jnp.dot(latent_rows, value_weight, preferred_element_type=jnp.float32).astype(
            jnp.bfloat16
        )
        return (
            keys.reshape(count, heads, PLAIN_DIM),
            values.reshape(count, heads, VALUE_DIM),
            key_rows,
        )

    def add_keys(carry, unpacked, start):
        total, highest = carry
        keys, values, rotated_rows = unpacked
        count = keys.shape[0]
        scores = jnp.einsum("qhd,khd->qhk", queries, keys, preferred_element_type=jnp.float32)
        scores = scores + jnp.einsum(
            "qhr,kr->qhk", query_rotated, rotated_rows, preferred_element_type=jnp.float32
        )
        scores = scores * factor
        key_positions = start + jnp.arange(count, dtype=jnp.int32)
        allowed = (key_positions[None, :] <= positions[:, None])[:, None, :]
        masked = jnp.where(allowed, scores, -1e30)
        newest = jnp.maximum(highest, jnp.max(masked, axis=-1))
        weights = jnp.where(allowed, jnp.exp(masked - newest[..., None]), 0.0).astype(jnp.bfloat16)
        total = total * jnp.exp(highest - newest)[..., None] + jnp.einsum(
            "qhk,khd->qhd", weights, values, preferred_element_type=jnp.float32
        )
        return (total, newest)

    def make_fold(unpack):

        def guarded(carry, piece, start):

            def compute(state):
                return add_keys(state, unpack(piece), start)

            def keep(state):
                return state

            return lax.cond(start > last_position, keep, compute, carry)

        def fold(carry, piece, start):
            count = piece[0].shape[0]
            if count > key_span and count % key_span == 0:

                def step(index, inner):
                    begin = index * key_span
                    sliced = tuple(
                        (lax.dynamic_slice_in_dim(member, begin, key_span, 0) for member in piece)
                    )
                    return guarded(inner, sliced, start + begin)

                return lax.fori_loop(0, count // key_span, step, carry)
            return guarded(carry, piece, start)

        return fold

    initial = (
        jnp.zeros((tokens, heads, VALUE_DIM), jnp.float32),
        jnp.full((tokens, heads), -1e30, jnp.float32),
    )
    folded = make_fold(expand_latent)(
        initial,
        (
            lax.all_gather(latent, "ep", axis=0, tiled=True),
            lax.all_gather(key_rotated, "ep", axis=0, tiled=True),
        ),
        jnp.int32(0),
    )
    context = folded[0]
    head_output = (
        normalize(context, head_gain.reshape(heads, VALUE_DIM))
        .astype(jnp.bfloat16)
        .reshape(tokens, heads * VALUE_DIM)
    )
    return lax.psum_scatter(
        rounded(jnp.dot(head_output, out_weight, preferred_element_type=jnp.float32)).astype(
            jnp.bfloat16
        ),
        "tp",
        scatter_dimension=0,
        tiled=True,
    )


def experts(expert_input, expert_gain, routes, route_weight, gate_weight, up_weight, down_weight):
    tokens = expert_input.shape[0]
    features = expert_input.shape[1]
    count_ep = lax.axis_size("ep")
    capacity = min(tokens, max(2, (9 * tokens + 4 * count_ep - 1) // (4 * count_ep)))
    normed = normalize(expert_input, expert_gain).astype(jnp.bfloat16)
    chosen = routes.reshape(-1)
    onehot = (chosen[:, None] == jnp.arange(count_ep, dtype=jnp.int32)[None, :]).astype(jnp.int32)
    ranks = jnp.sum(jnp.cumsum(onehot, axis=0) * onehot, axis=1) - 1
    destination = chosen * capacity + ranks
    outgoing = (
        jnp.zeros((count_ep * capacity, features), jnp.bfloat16)
        .at[destination]
        .set(jnp.repeat(normed, TOP, axis=0))
    )
    gate_local = gate_weight[0]
    up_local = up_weight[0]
    down_local = down_weight[0]
    arrived = lax.all_to_all(outgoing, "ep", split_axis=0, concat_axis=0, tiled=True)
    piece = lax.all_gather(arrived, "tp", axis=0, tiled=True)
    gate = jnp.dot(piece, gate_local, preferred_element_type=jnp.float32)
    upward = jnp.dot(piece, up_local, preferred_element_type=jnp.float32)
    hidden = (jax.nn.silu(gate) * upward).astype(jnp.bfloat16)
    summed = lax.psum_scatter(
        rounded(jnp.dot(hidden, down_local, preferred_element_type=jnp.float32)).astype(
            jnp.bfloat16
        ),
        "tp",
        scatter_dimension=0,
        tiled=True,
    )
    returned = lax.all_to_all(summed, "ep", split_axis=0, concat_axis=0, tiled=True)
    picked = returned[destination].astype(jnp.float32).reshape(tokens, TOP, features)
    combined = jnp.sum(picked * route_weight[:, :, None], axis=1)
    return combined.astype(jnp.bfloat16)


def body(
    query_plain,
    query_rotary,
    latent_input,
    rotary_key,
    key_weight,
    value_weight,
    latent_gain,
    head_gain,
    out_weight,
    expert_input,
    expert_gain,
    routes,
    route_weight,
    gate_weight,
    up_weight,
    down_weight,
):
    attended = attend(
        query_plain,
        query_rotary,
        latent_input,
        rotary_key,
        key_weight,
        value_weight,
        latent_gain,
        head_gain,
        out_weight,
    )
    expert_out = experts(
        expert_input, expert_gain, routes, route_weight, gate_weight, up_weight, down_weight
    )
    return (attended, expert_out)


def solution(mesh):
    return jax.shard_map(
        body,
        mesh=mesh,
        in_specs=(
            P(("grp", "ep"), "tp"),
            P(("grp", "ep"), "tp"),
            P(("grp", "ep"), None),
            P(("grp", "ep"), None),
            P(None, "tp"),
            P(None, "tp"),
            P(),
            P("tp"),
            P("tp", None),
            P(("grp", "ep", "tp"), None),
            P(),
            P(("grp", "ep", "tp"), None),
            P(("grp", "ep", "tp"), None),
            P("ep", None, "tp"),
            P("ep", None, "tp"),
            P("ep", "tp", None),
        ),
        out_specs=(P(("grp", "ep", "tp"), None), P(("grp", "ep", "tp"), None)),
        check_vma=False,
    )
```

profile of v0, /device:TPU:0, one launch (start us, length us, event | category | flops | bytes accessed | tf_op | source)
XLA Modules:
  0.0 206.0 jit_solution(753262045662705016)
XLA Ops:
  7.2 0.8 copy.42
  8.3 0.7 broadcast_multiply_fusion
  9.0 1.2 reduce-window.6
  10.9 0.7 convert_element_type.111
  11.6 1.2 fusion.15
  12.8 1.2 fusion.17
  14.1 0.6 broadcast_in_dim.37
  15.2 2.5 %scatter_custom_fusion = bf16[288,2048]{1,0:T(8,128)(2,1)S(1)} fusion(s32[256]{0:T(256)S(1)} %bitcast.83, bf16[256,2048]{1,0:T(8,128)(2,1)S(1)} %reshape.290, bf16[]{:T(256)} %constant.59.clone.1), kind=kCustom, calls=%fused_computation.34 | custom fusion | bytes 1179650 | tf_op jit(solution)/shard_map/scatter | solution.py:168
  17.6 34.8 %all_to_all.24 = bf16[4,72,2048]{2,1,0:T(8,128)(2,1)} all-to-all(bf16[4,72,2048]{2,1,0:T(8,128)(2,1)S(1)} %bitcast.75), channel_id=1, replica_groups=mesh['grp'=2,'ep'=4,'tp'=4] {'ep'}, dimensions={0} | all-to-all | bytes 2359296 | tf_op jit(solution)/shard_map/all_to_all | solution.py:173
  52.5 36.6 %all-gather.2.cloned.1.call-done = bf16[1152,2048]{1,0:T(8,128)(2,1)} async-done(((bf16[288,2048]{1,0:T(8,128)(2,1)}), bf16[1152,2048]{1,0:T(8,128)(2,1)}) %all-gather.2.cloned.1.call-update) | async-done | bytes 4718608 | tf_op jit(solution)/shard_map/all_gather | solution.py:174
  89.2 8.1 %fusion.10 = f32[1152,896]{1,0:T(8,128)S(1)} fusion(bf16[1152,2048]{1,0:T(8,128)(2,1)} %all-gather.2.cloned.1.call-done, bf16[1,2048,896]{2,1,0:T(8,128)(2,1)} %param.31), kind=kOutput, calls=%fused_computation.24 | convolution fusion | flops 4227858432 | bytes 12517376 | tf_op jit(solution)/shard_map/dot_general | solution.py:175
  97.3 5.4 %fusion.12 = bf16[1152,896]{1,0:T(8,128)(2,1)S(1)} fusion(bf16[1152,2048]{1,0:T(8,128)(2,1)S(1)} %copy-done.8, bf16[1,2048,896]{2,1,0:T(8,128)(2,1)S(1)} %copy-done.9, f32[1152,896]{1,0:T(8,128)S(1)} %fusion.10), kind=kOutput, calls=%fused_computation.26 | convolution fusion | flops 4234051584 | bytes 14581760 | tf_op jit(solution)/shard_map/dot_general | solution.py:176
  102.7 6.7 %convolution_convert_fusion.2 = bf16[1152,2048]{1,0:T(8,128)(2,1)} fusion(bf16[1152,896]{1,0:T(8,128)(2,1)S(1)} %fusion.12, bf16[1,896,2048]{2,1,0:T(8,128)(2,1)S(1)} %copy-done.10), kind=kOutput, calls=%fused_computation.20 | convolution fusion | flops 4230217728 | bytes 10452992 | tf_op jit(solution)/shard_map/dot_general | solution.py:179
  110.4 13.2 %all_gather.10 = bf16[1024,32]{0,1:T(8,128)(2,1)S(1)} all-gather(bf16[256,32]{0,1:T(8,128)(2,1)S(1)} %pad_maximum_fusion.1), channel_id=1, replica_groups=mesh['grp'=2,'ep'=4,'tp'=4] {'ep'}, dimensions={0}, use_global_device_ids=true | all-gather | bytes 81920 | tf_op jit(solution)/shard_map/all_gather | solution.py:135
  124.1 16.2 %all_gather.9 = bf16[1024,256]{1,0:T(8,128)(2,1)S(1)} all-gather(bf16[256,256]{1,0:T(8,128)(2,1)S(1)} %fusion.22), channel_id=1, replica_groups=mesh['grp'=2,'ep'=4,'tp'=4] {'ep'}, dimensions={0}, use_global_device_ids=true | all-gather | bytes 655360 | tf_op jit(solution)/shard_map/all_gather | solution.py:134
  140.3 2.5 %conditional.1 = (f32[256,2,64]{0,2,1:T(8,128)S(1)}, f32[256,2,1]{0,1,2:T(2,128)S(1)}) conditional(s32[]{:T(128)} %convert_element_type.96, (s32[]{:T(128)}, s32[256]{0:T(256)S(1)}, bf16[1024,256]{1,0:T(8,128)(2,1)S(1)}, bf16[256,128]{1,0:T(8,128)(2,1)S(1)}, bf16[256,128]{1,0:T(8,128)(2,1)S(1)}, /*index=5*/bf16[256,2,32]{0,2,1:T(8,128)(2,1)S(1)}, ...), branch_computations={%region_1.0_spmd, %region_4.5_spmd} | conditional | flops 306283264 | bytes 11846676 | solution.py:109
  141.4 0.6 fusion.39
  142.9 1.5 convolution_convert_fusion.3
  144.4 13.3 %reduce-scatter.5.cloned.1.call-done = bf16[288,2048]{1,0:T(8,128)(2,1)} async-done(((bf16[1152,2048]{1,0:T(8,128)(2,1)}), bf16[288,2048]{1,0:T(8,128)(2,1)}) %reduce-scatter.5.cloned.1.call-update) | async-done | bytes 1179664 | tf_op jit(solution)/shard_map/reduce_scatter | solution.py:178
  157.7 4.6 %all-to-all-start.1 = ((bf16[4,72,2048]{2,1,0:T(8,128)(2,1)}), bf16[4,72,2048]{2,1,0:T(8,128)(2,1)S(1)}, u32[]{:S(2)}, u32[]{:S(2)}) async-start(bf16[4,72,2048]{2,1,0:T(8,128)(2,1)} %bitcast.76), calls=%async_computation.3 | async-start | bytes 2359296 | tf_op jit(solution)/shard_map/all_to_all | solution.py:186
  162.4 28.3 %all-to-all-done.1 = bf16[4,72,2048]{2,1,0:T(8,128)(2,1)S(1)} async-done(((bf16[4,72,2048]{2,1,0:T(8,128)(2,1)}), bf16[4,72,2048]{2,1,0:T(8,128)(2,1)S(1)}, u32[]{:S(2)}, u32[]{:S(2)}) %all-to-all-start.1) | async-done | bytes 1179680 | tf_op jit(solution)/shard_map/all_to_all | solution.py:186
  190.7 2.3 %gather_fusion = bf16[256,2048]{1,0:T(8,128)(2,1)} fusion(bf16[288,2048]{1,0:T(8,128)(2,1)S(1)} %bitcast.73, s32[1024]{0:T(1024)S(1)} %pad_clamp_fusion), kind=kCustom, calls=%fused_computation | custom fusion | bytes 2098176 | tf_op jit(solution)/shard_map/gather | solution.py:187
  193.0 2.4 %reshape.277 = f32[128,2,2048]{2,1,0:T(2,128)S(1)} reshape(bf16[256,2048]{1,0:T(8,128)(2,1)} %gather_fusion) | data formatting | bytes 3145728 | tf_op jit(solution)/shard_map/convert_element_type | solution.py:187
  195.4 4.0 %multiply_reduce_fusion.1 = bf16[128,2048]{1,0:T(8,128)(2,1)} fusion(f32[128,2,2048]{2,1,0:T(2,128)S(1)} %reshape.277, f32[128,2]{1,0:T(8,128)S(1)} %copy.46), kind=kLoop, calls=%fused_computation.28 | loop fusion | flops 786432 | bytes 2622464 | tf_op jit(solution)/shard_map/reduce_sum | solution.py:188
  (74 shorter events, 4.9 us)
Async XLA Ops:
  7.2 135.7 %copy-start = (bf16[128,2048]{1,0:T(8,128)(2,1)S(1)}, bf16[128,2048]{1,0:T(8,128)(2,1)}, u32[]{:S(2)}) copy-start(bf16[128,2048]{1,0:T(8,128)(2,1)} %param.26) | copy-start | bytes 1572868
  7.2 82.0 %all-gather.2.cloned.1.call-start = ((), (), s32[]{:S(2)}) async-start(), calls=%async_computation.5 | async-start | bytes 5898240 | tf_op jit(solution)/shard_map/all_gather | solution.py:174
  52.5 105.2 %reduce-scatter.5.cloned.1.call-start = ((), (), s32[]{:S(2)}) async-start(), calls=%async_computation.6 | async-start | bytes 5898240 | tf_op jit(solution)/shard_map/reduce_scatter | solution.py:178
  89.1 8.1 %copy-start.8 = (bf16[1152,2048]{1,0:T(8,128)(2,1)S(1)}, bf16[1152,2048]{1,0:T(8,128)(2,1)}, u32[]{:S(2)}) copy-start(bf16[1152,2048]{1,0:T(8,128)(2,1)} %all-gather.2.cloned.1.call-done) | copy-start | bytes 14155780
  89.1 8.1 %copy-start.9 = (bf16[1,2048,896]{2,1,0:T(8,128)(2,1)S(1)}, bf16[1,2048,896]{2,1,0:T(8,128)(2,1)}, u32[]{:S(2)}) copy-start(bf16[1,2048,896]{2,1,0:T(8,128)(2,1)} %param.32) | copy-start | bytes 11010052
  97.3 5.4 %copy-start.10 = (bf16[1,896,2048]{2,1,0:T(8,128)(2,1)S(1)}, bf16[1,896,2048]{2,1,0:T(8,128)(2,1)}, u32[]{:S(2)}) copy-start(bf16[1,896,2048]{2,1,0:T(8,128)(2,1)} %param.33) | copy-start | bytes 11010052
  109.4 0.7 copy-start.11
  109.4 0.7 copy-start.12
  109.4 0.8 copy-start.6
  109.4 14.3 %copy-start.5 = (bf16[256,64]{0,1:T(8,128)(2,1)S(1)}, bf16[256,64]{0,1:T(8,128)(2,1)}, u32[]{:S(2)}) copy-start(bf16[256,64]{0,1:T(8,128)(2,1)} %param.19) | copy-start | bytes 98308
  109.4 14.4 %copy-start.1 = (bf16[256,256]{1,0:T(8,128)(2,1)S(1)}, bf16[256,256]{1,0:T(8,128)(2,1)}, u32[]{:S(2)}) copy-start(bf16[256,256]{1,0:T(8,128)(2,1)} %param.20) | copy-start | bytes 393220
  109.5 30.8 %copy-start.2 = (bf16[256,128]{1,0:T(8,128)(2,1)S(1)}, bf16[256,128]{1,0:T(8,128)(2,1)}, u32[]{:S(2)}) copy-start(bf16[256,128]{1,0:T(8,128)(2,1)} %param.18) | copy-start | bytes 196612
  109.5 30.8 %copy-start.3 = (bf16[256,128]{1,0:T(8,128)(2,1)S(1)}, bf16[256,128]{1,0:T(8,128)(2,1)}, u32[]{:S(2)}) copy-start(bf16[256,128]{1,0:T(8,128)(2,1)} %param.22) | copy-start | bytes 196612
  109.5 30.8 %copy-start.4 = (bf16[256,128]{1,0:T(8,128)(2,1)S(1)}, bf16[256,128]{1,0:T(8,128)(2,1)}, u32[]{:S(2)}) copy-start(bf16[256,128]{1,0:T(8,128)(2,1)} %param.23) | copy-start | bytes 196612
  109.5 89.9 %reduce-scatter.3.cloned.1.call-start = ((), (), s32[]{:S(2)}) async-start(), calls=%async_computation.4 | async-start | bytes 1310720 | tf_op jit(solution)/shard_map/reduce_scatter | solution.py:145
  144.4 17.9 %copy-start.7 = (f32[128,2]{0,1:T(2,128)S(1)}, f32[128,2]{0,1:T(2,128)}, u32[]{:S(2)}) copy-start(f32[128,2]{0,1:T(2,128)} %param.30) | copy-start | bytes 3076
  157.7 33.0 %all-to-all-start.1 = ((bf16[4,72,2048]{2,1,0:T(8,128)(2,1)}), bf16[4,72,2048]{2,1,0:T(8,128)(2,1)S(1)}, u32[]{:S(2)}, u32[]{:S(2)}) async-start(bf16[4,72,2048]{2,1,0:T(8,128)(2,1)} %bitcast.76), calls=%async_computation.3 | async-start | bytes 2359296 | tf_op jit(solution)/shard_map/all_to_all | solution.py:186
Sparse Core Ops, SparseCore 0:
  52.6 36.5 all-gather.1
  109.6 47.9 reduce-scatter.4
  160.8 24.7 reduce-scatter.2
where the time goes:
time: 206 us
  waiting for transfers between devices  78.2 us (38%)
  blocking collectives  64.2 us (31%)
  matrix products  23.8 us (12%)
  between operations  14 us (7%)
  local copies, waits for them, and re-layouts  10.8 us (5%)
  other arithmetic  10.1 us (5%)
  starting transfers between devices  4.73 us (2%)
    all_gather x1, waiting for transfers between devices, experts(): piece = lax.all_gather(arrived, 'tp', axis=0, tiled=True)  36.6 us
    all_to_all x1, blocking collectives, experts(): lax.all_to_all(outgoing, 'ep', split_axis=0, concat_axis=0, tiled=True)  34.8 us
    all_to_all x1, waiting for transfers between devices, experts(): lax.all_to_all(summed, 'ep', split_axis=0, concat_axis=0, tiled=True)  28.3 us
    all_gather x1, blocking collectives, attend(): lax.all_gather(latent, 'ep', axis=0, tiled=True)  16.2 us
    reduce_scatter x1, waiting for transfers between devices, experts(): lax.psum_scatter(rounded(jnp.dot(hidden, down_local, preferred_element_ty...  13.3 us
    all_gather x1, blocking collectives, attend(): lax.all_gather(key_rotated, 'ep', axis=0, tiled=True)  13.2 us
    dot_general x1, matrix products, experts(): gate = jnp.dot(piece, gate_local, preferred_element_type=jnp.float32)  8.11 us
    dot_general x1, matrix products, experts(): jnp.dot(hidden, down_local, preferred_element_type=jnp.float32)  6.71 us
  transfers between devices with their start and end apart: 4, of which 3 were waited for; matrix products, arithmetic and copies ran while one was open for 7% of the time, Pallas kernels for 0%

commit v1 on v0

v1 whole, which is shorter than its diff:
```python
import functools
import jax
import jax.numpy as jnp
from jax import lax
from jax.experimental import pallas as pl
from jax.experimental.pallas import tpu as pltpu
from jax.sharding import PartitionSpec as P

PLAIN_DIM = 64
ROTARY_DIM = 32
VALUE_DIM = 64
EPSILON = 1e-06
THETA = 10000.0
LOWEST = -1e30
LANES = 128
MESH = pl.DeviceIdType.MESH
F32 = jnp.float32
BF16 = jnp.bfloat16


def normalize(entries, gain):
    wide = entries.astype(F32)
    factor = lax.rsqrt(jnp.mean(wide * wide, axis=-1, keepdims=True) + EPSILON)
    return wide * factor * gain.astype(F32)


def rotate(entries, positions):
    half = entries.shape[-1] // 2
    freqs = THETA ** (-jnp.arange(half, dtype=F32) / half)
    angle = positions.astype(F32)[:, None, None] * freqs[None, None, :]
    cosine = jnp.cos(angle)
    sine = jnp.sin(angle)
    first = entries[..., :half].astype(F32)
    second = entries[..., half:].astype(F32)
    turned = jnp.concatenate(
        [first * cosine - second * sine, first * sine + second * cosine], axis=-1
    )
    return turned.astype(BF16)


def kernel(
    dims,
    x_ref, gain_ref, routes_ref, weight_ref, lat_ref, q_ref, qr_ref, kw_ref, vw_ref,
    hgain_ref, ow_ref, gate_hbm, up_hbm, down_hbm,
    att_ref, out_ref,
    wgu, wd, outgo, rows, part, hidden, near, pair, across, done, back,
    lats, total, highest, head_part, head_near, head_pair, head_across,
    w_sem, z_send, z_recv, fx_send, fx_recv, fc_send, fc_recv, fd_send, fd_recv,
    n_send, n_recv, a_send, a_recv, b_send, b_recv,
    lz_send, lz_recv, lx_send, lx_recv, lc_send, lc_recv, ld_send, ld_recv,
    h_send, h_recv, i_send, i_recv,
):
    n_ep, n_tp, cap = dims
    tokens = x_ref.shape[0]
    features = x_ref.shape[1]
    tiles = wgu.shape[0]
    pitch = rows.shape[2]
    outer = n_tp // 2
    e = lax.axis_index("ep")
    t = lax.axis_index("tp")
    core = lax.rem(t, 2)
    side = t // 2
    mate = t + 1 - 2 * core
    over = lax.rem(t + 2, n_tp)
    mine = core * outer + side
    mine_over = core * outer + (1 - side)
    sent = pl.ds(0, cap)

    def peer(k):
        return lax.bitwise_xor(e, k)

    def remote(src, dst, send, recv, where):
        return pltpu.make_async_remote_copy(
            src_ref=src, dst_ref=dst, send_sem=send, recv_sem=recv,
            device_id=where, device_id_type=MESH,
        )

    def tile_copies(n):
        columns = pl.ds(n * LANES, LANES)
        return (
            pltpu.make_async_copy(
                gate_hbm.at[0, :, columns], wgu.at[n, :, pl.ds(0, LANES)], w_sem.at[2 * n]
            ),
            pltpu.make_async_copy(
                up_hbm.at[0, :, columns], wgu.at[n, :, pl.ds(LANES, LANES)], w_sem.at[2 * n + 1]
            ),
        )

    down_copy = pltpu.make_async_copy(down_hbm.at[0], wd, w_sem.at[2 * tiles])
    for n in range(tiles):
        for copy in tile_copies(n):
            copy.start()
    down_copy.start()

    barrier = pltpu.get_barrier_semaphore()

    @pl.loop(1, n_ep)
    def _(k):
        pl.semaphore_signal(barrier, inc=1, device_id={"ep": peer(k)}, device_id_type=MESH)

    for where in (mate, over):
        pl.semaphore_signal(barrier, inc=1, device_id={"tp": where}, device_id_type=MESH)
    pl.semaphore_wait(barrier, n_ep + 1)

    def lat_z(k, slot):
        return remote(lat_ref, lats.at[slot, t], lz_send.at[k], lz_recv.at[k], {"ep": peer(k)})

    def lat_x(s, src):
        return remote(src, lats.at[s, t], lx_send.at[s], lx_recv.at[s], {"tp": over})

    def lat_c(s, src):
        return remote(src, lats.at[s, t], lc_send.at[s], lc_recv.at[s], {"tp": mate})

    def lat_d(s):
        return remote(
            lats.at[s, over], lats.at[s, over], ld_send.at[s], ld_recv.at[s], {"tp": mate}
        )

    @pl.loop(1, n_ep)
    def _(k):
        lat_z(k, e).start()

    lat_x(e, lat_ref).start()
    lat_c(e, lat_ref).start()
    lats[e, t] = lat_ref[...]

    wide = x_ref[...].astype(F32)
    factor = lax.rsqrt(jnp.mean(wide * wide, axis=-1, keepdims=True) + EPSILON)
    normed = (wide * factor * gain_ref[...].astype(F32)).astype(BF16)
    before = lax.broadcasted_iota(jnp.int32, (tokens, tokens), 0)
    after = lax.broadcasted_iota(jnp.int32, (tokens, tokens), 1)
    upper = jnp.where(before <= after, 1.0, 0.0).astype(BF16)

    def selection(j):
        named = (routes_ref[0:1, :] == j) | (routes_ref[1:2, :] == j)
        member = jnp.where(named, 1.0, 0.0)
        wide_member = jnp.broadcast_to(member, (8, tokens)).astype(BF16)
        ranks = jnp.dot(wide_member, upper, preferred_element_type=F32)[0:1, :]
        ranks = jnp.where(named, ranks, 0.0)
        places = lax.broadcasted_iota(jnp.int32, (cap, tokens), 0).astype(F32) + 1.0
        return jnp.where(places == ranks, 1.0, 0.0)

    def z_copy(k, slot):
        return remote(
            outgo.at[k, sent], rows.at[slot, mine, sent], z_send.at[k], z_recv.at[k],
            {"ep": peer(k)},
        )

    def picked_rows(j):
        return jnp.dot(selection(j).astype(BF16), normed, preferred_element_type=F32).astype(BF16)

    def forward_x(s):
        block = rows.at[s, mine, sent]
        return remote(block, block, fx_send.at[s], fx_recv.at[s], {"tp": over})

    def forward_c(s):
        block = rows.at[s, mine, sent]
        return remote(block, block, fc_send.at[s], fc_recv.at[s], {"tp": mate})

    def forward_d(s):
        block = rows.at[s, mine_over, sent]
        return remote(block, block, fd_send.at[s], fd_recv.at[s], {"tp": mate})

    @pl.loop(1, n_ep)
    def _(k):
        outgo[k, sent] = picked_rows(peer(k))
        z_copy(k, e).start()

    rows[e, mine, sent] = picked_rows(e)

    def head_mask(width, h, rows_count):
        lane = lax.broadcasted_iota(jnp.int32, (rows_count, width * heads), 1)
        return (lane >= h * width) & (lane < (h + 1) * width)

    heads = kw_ref.shape[1] // PLAIN_DIM
    queries = q_ref.shape[0]
    quarter = lat_ref.shape[0]
    latent_width = kw_ref.shape[0]
    rotary_width = heads * ROTARY_DIM
    scale = (PLAIN_DIM + ROTARY_DIM) ** (-0.5)

    def head_c():
        return remote(head_part.at[1 - core], head_near, h_send, h_recv, {"tp": mate})

    def head_x():
        return remote(head_pair, head_across, i_send, i_recv, {"tp": over})

    def attend():
        @pl.loop(1, n_ep)
        def _(k):
            s = peer(k)
            lat_z(k, s).wait_recv()
            lat_x(s, lats.at[s, t]).start()
            lat_c(s, lats.at[s, t]).start()

        @pl.loop(0, n_ep)
        def _(k):
            s = peer(k)
            lat_x(s, lats.at[s, t]).wait_recv()
            lat_d(s).start()

        @pl.loop(0, n_ep)
        def _(k):
            s = peer(k)
            lat_c(s, lats.at[s, t]).wait_recv()
            lat_d(s).wait_recv()

        total[...] = jnp.zeros_like(total)
        highest[...] = jnp.full_like(highest, LOWEST)

        @pl.loop(0, n_ep)
        def _(s):
            @pl.when(s <= e)
            def _():
                piece = lats[s].reshape(n_tp * quarter, lat_ref.shape[1])
                latent = piece[:, :latent_width]
                turned = piece[:, latent_width : latent_width + rotary_width]
                keys = jnp.dot(latent, kw_ref[...], preferred_element_type=F32).astype(BF16)
                values = jnp.dot(latent, vw_ref[...], preferred_element_type=F32).astype(BF16)
                shape = (queries, n_tp * quarter)
                at_query = e * queries + lax.broadcasted_iota(jnp.int32, shape, 0)
                at_key = s * queries + lax.broadcasted_iota(jnp.int32, shape, 1)
                allowed = at_key <= at_query
                for h in range(heads):
                    plain = jnp.where(head_mask(PLAIN_DIM, h, queries), q_ref[...].astype(F32), 0.0).astype(BF16)
                    rot = jnp.where(head_mask(ROTARY_DIM, h, queries), qr_ref[...].astype(F32), 0.0).astype(BF16)
                    contract = (((1,), (1,)), ((), ()))
                    scores = lax.dot_general(plain, keys, contract, preferred_element_type=F32)
                    scores += lax.dot_general(rot, turned, contract, preferred_element_type=F32)
                    masked = jnp.where(allowed, scores * scale, LOWEST)
                    old = highest[h]
                    new = jnp.maximum(old, jnp.max(masked, axis=-1, keepdims=True))
                    weights = jnp.where(allowed, jnp.exp(masked - new[:, 0:1]), 0.0).astype(BF16)
                    total[h] = total[h] * jnp.exp(old - new) + jnp.dot(
                        weights, values, preferred_element_type=F32
                    )
                    highest[h] = new

        context = jnp.zeros((queries, heads * VALUE_DIM), F32)
        for h in range(heads):
            inside = head_mask(VALUE_DIM, h, queries)
            own = jnp.where(inside, total[h], 0.0)
            square = jnp.sum(own * own, axis=-1, keepdims=True) * (1.0 / VALUE_DIM)
            context = context + own * lax.rsqrt(square + EPSILON)
        head_output = (context * hgain_ref[...].astype(F32)).astype(BF16)
        share = jnp.dot(head_output, ow_ref[...], preferred_element_type=F32).astype(BF16)
        for other in range(n_tp):
            head_part[other % 2, other // 2] = share[other * quarter : (other + 1) * quarter]
        head_c().start()

    def multiply(s):
        piece = rows.at[s]
        stacked = n_tp * pitch

        @pl.loop(0, tiles)
        def _(n):
            both = jnp.dot(
                piece[...].reshape(stacked, features), wgu[n], preferred_element_type=F32
            )
            gate = both[:, :LANES]
            hidden[:, pl.ds(pl.multiple_of(n * LANES, LANES), LANES)] = (
                gate / (1.0 + jnp.exp(-gate)) * both[:, LANES:]
            ).astype(BF16)

        step = 2 * LANES

        @pl.loop(0, features // step)
        def _(n):
            columns = pl.ds(pl.multiple_of(n * step, step), step)
            result = jnp.dot(hidden[...], wd[:, columns], preferred_element_type=F32)
            part[s, :, :, :, columns] = result.astype(BF16).reshape(2, outer, pitch, step)

    def near_copy(s):
        return remote(
            part.at[s, 1 - core, :, sent], near.at[s, :, sent], n_send.at[s], n_recv.at[s],
            {"tp": mate},
        )

    def across_copy(s):
        return remote(
            pair.at[s, sent], across.at[s, sent], a_send.at[s], a_recv.at[s], {"tp": over}
        )

    def back_copy(k, slot):
        s = peer(k)
        return remote(
            done.at[s, sent], back.at[slot, sent], b_send.at[k], b_recv.at[k], {"ep": s}
        )

    @pl.loop(0, n_ep + 5)
    def _(it):
        @pl.when((it >= 2) & (it < n_ep + 2))
        def _():
            s = peer(it - 2)
            forward_c(s).wait_recv()
            forward_d(s).wait_recv()

            @pl.when(it == 2)
            def _():
                for n in range(tiles):
                    for copy in tile_copies(n):
                        copy.wait()
                down_copy.wait()

            multiply(s)
            near_copy(s).start()

        @pl.when((it >= 3) & (it < n_ep + 3))
        def _():
            s = peer(it - 3)
            near_copy(s).wait_recv()
            pair[s, sent] = (
                part[s, core, 1 - side, sent].astype(F32) + near[s, 1 - side, sent].astype(F32)
            ).astype(BF16)
            across_copy(s).start()

        @pl.when(it == 2)
        def _():
            head_c().wait_recv()
            head_pair[...] = (
                head_part[core, 1 - side].astype(F32) + head_near[1 - side].astype(F32)
            ).astype(BF16)
            head_x().start()

        @pl.when((it >= 1) & (it < n_ep + 1))
        def _():
            s = peer(it - 1)
            forward_x(s).wait_recv()
            forward_d(s).start()

        @pl.when((it >= 4) & (it < n_ep + 4))
        def _():
            k = it - 4
            s = peer(k)
            across_copy(s).wait_recv()
            final = (
                part[s, core, side, sent].astype(F32)
                + near[s, side, sent].astype(F32)
                + across[s, sent].astype(F32)
            ).astype(BF16)

            @pl.when(k == 0)
            def _():
                back[e, sent] = final

            @pl.when(k > 0)
            def _():
                done[s, sent] = final
                back_copy(k, e).start()

        @pl.when(it < n_ep)
        def _():
            s = peer(it)

            @pl.when(it > 0)
            def _():
                z_copy(it, s).wait_recv()

            forward_x(s).start()
            forward_c(s).start()

        @pl.when(it == 0)
        def _():
            attend()

    head_x().wait_recv()
    att_ref[...] = (
        head_part[core, side].astype(F32)
        + head_near[side].astype(F32)
        + head_across[...].astype(F32)
    ).astype(BF16)

    def gathered(k, acc):
        s = peer(k)

        @pl.when(k > 0)
        def _():
            back_copy(k, s).wait_recv()

        scaled = jnp.where(routes_ref[0:1, :] == s, weight_ref[0:1, :], 0.0)
        scaled = scaled + jnp.where(routes_ref[1:2, :] == s, weight_ref[1:2, :], 0.0)
        spread = selection(s) * scaled
        high = spread.astype(BF16)
        low = (spread - high.astype(F32)).astype(BF16)
        contract = (((0,), (0,)), ((), ()))
        block = back[s, sent]
        acc[...] += lax.dot_general(high, block, contract, preferred_element_type=F32)
        acc[...] += lax.dot_general(low, block, contract, preferred_element_type=F32)

    def combine(acc):
        acc[...] = jnp.zeros_like(acc)

        @pl.loop(0, n_ep)
        def _(k):
            gathered(k, acc)

        out_ref[...] = acc[...].astype(BF16)

    pl.run_scoped(combine, pltpu.VMEM((tokens, features), F32))

    @pl.loop(0, n_ep)
    def _(k):
        s = peer(k)

        @pl.when(k > 0)
        def _():
            z_copy(k, e).wait_send()
            lat_z(k, e).wait_send()
            back_copy(k, e).wait_send()

        forward_x(s).wait_send()
        forward_c(s).wait_send()
        forward_d(s).wait_send()
        near_copy(s).wait_send()
        across_copy(s).wait_send()
        lat_x(s, lats.at[s, t]).wait_send()
        lat_c(s, lats.at[s, t]).wait_send()
        lat_d(s).wait_send()

    head_c().wait_send()
    head_x().wait_send()


def body(
    query_plain, query_rotary, latent_input, rotary_key, key_weight, value_weight, latent_gain,
    head_gain, out_weight, expert_input, expert_gain, routes, route_weight, gate_weight,
    up_weight, down_weight,
):
    n_ep, n_tp = lax.axis_size("ep"), lax.axis_size("tp")
    e, t = lax.axis_index("ep"), lax.axis_index("tp")
    tokens, features = expert_input.shape
    count = query_plain.shape[0]
    quarter = count // n_tp
    heads = key_weight.shape[1] // PLAIN_DIM
    capacity = min(tokens, max(2, (9 * tokens + 4 * n_ep - 1) // (4 * n_ep)))
    cap = -(-capacity // 8) * 8
    pitch = -(-cap // 16) * 16
    units = gate_weight.shape[2]
    tiles = units // LANES

    own = lax.dynamic_slice_in_dim(latent_input, t * quarter, quarter, 0)
    own_key = lax.dynamic_slice_in_dim(rotary_key, t * quarter, quarter, 0)
    own_positions = e * count + t * quarter + jnp.arange(quarter, dtype=jnp.int32)
    latent = normalize(own, latent_gain).astype(BF16)
    turned = rotate(own_key.reshape(quarter, 1, ROTARY_DIM), own_positions).reshape(
        quarter, ROTARY_DIM
    )
    width = latent.shape[1] + heads * ROTARY_DIM
    padded = -(-width // LANES) * LANES
    packed = jnp.concatenate(
        [latent] + [turned] * heads + [jnp.zeros((quarter, padded - width), BF16)], axis=1
    )
    positions = e * count + jnp.arange(count, dtype=jnp.int32)
    query_rotated = rotate(query_rotary.reshape(count, heads, ROTARY_DIM), positions).reshape(
        count, heads * ROTARY_DIM
    )

    dma = pltpu.SemaphoreType.DMA
    vmem = pl.BlockSpec(memory_space=pltpu.VMEM)
    far = pl.BlockSpec(memory_space=pl.ANY)
    outer = n_tp // 2
    block = (pitch, features)
    attended, expert_out = pl.pallas_call(
        functools.partial(kernel, (n_ep, n_tp, cap)),
        out_shape=(
            jax.ShapeDtypeStruct((quarter, features), BF16),
            jax.ShapeDtypeStruct((tokens, features), BF16),
        ),
        in_specs=[vmem] * 11 + [far] * 3,
        out_specs=(vmem, vmem),
        scratch_shapes=[
            pltpu.VMEM((tiles, features, 2 * LANES), BF16),
            pltpu.VMEM((units, features), BF16),
            pltpu.VMEM((n_ep,) + block, BF16),
            pltpu.VMEM((n_ep, n_tp) + block, BF16),
            pltpu.VMEM((n_ep, 2, outer) + block, BF16),
            pltpu.VMEM((n_tp * pitch, units), BF16),
            pltpu.VMEM((n_ep, outer) + block, BF16),
            pltpu.VMEM((n_ep,) + block, BF16),
            pltpu.VMEM((n_ep,) + block, BF16),
            pltpu.VMEM((n_ep,) + block, BF16),
            pltpu.VMEM((n_ep,) + block, BF16),
            pltpu.VMEM((n_ep, n_tp, quarter, padded), BF16),
            pltpu.VMEM((heads, count, heads * VALUE_DIM), F32),
            pltpu.VMEM((heads, count, LANES), F32),
            pltpu.VMEM((2, outer, quarter, features), BF16),
            pltpu.VMEM((outer, quarter, features), BF16),
            pltpu.VMEM((quarter, features), BF16),
            pltpu.VMEM((quarter, features), BF16),
            dma((2 * tiles + 1,)),
        ]
        + [dma((n_ep,))] * 22
        + [dma] * 4,
        compiler_params=pltpu.CompilerParams(
            collective_id=0, has_side_effects=True, vmem_limit_bytes=60 * 1024 * 1024
        ),
    )(
        expert_input, expert_gain.reshape(1, -1), routes.T, route_weight.T, packed,
        query_plain, query_rotated, key_weight, value_weight, head_gain.reshape(1, -1),
        out_weight, gate_weight, up_weight, down_weight,
    )
    return (attended, expert_out)


def solution(mesh):
    return jax.shard_map(
        body,
        mesh=mesh,
        in_specs=(
            P(("grp", "ep"), "tp"),
            P(("grp", "ep"), "tp"),
            P(("grp", "ep"), None),
            P(("grp", "ep"), None),
            P(None, "tp"),
            P(None, "tp"),
            P(),
            P("tp"),
            P("tp", None),
            P(("grp", "ep", "tp"), None),
            P(),
            P(("grp", "ep", "tp"), None),
            P(("grp", "ep", "tp"), None),
            P("ep", None, "tp"),
            P("ep", None, "tp"),
            P("ep", "tp", None),
        ),
        out_specs=(P(("grp", "ep", "tp"), None), P(("grp", "ep", "tp"), None)),
        check_vma=False,
    )
```

time: 206 us -> 114 us (0.55)
  the two profiles are of different devices: /device:TPU:0 before, /device:TPU:9 now
where the time goes in v1:
time: 114 us
  Pallas kernels  103 us (90%)
  local copies, waits for them, and re-layouts  6.49 us (6%)
  other arithmetic  3.49 us (3%)
    pallas_call x1, Pallas kernels, body(): pl.pallas_call(functools.partial(kernel, (n_ep, n_tp, cap)), out_shape=(j...  103 us
    unnamed x4, local copies, waits for them, and re-layouts  3.56 us

profile of v1, /device:TPU:9, one launch (start us, length us, event | category | flops | bytes accessed | tf_op | source)
XLA Modules:
  0.0 113.8 jit_solution(5230281839984414416)
XLA Ops:
  0.6 0.0 copy-start
  0.7 0.9 fusion
  1.6 0.7 convert_element_type.45
  2.2 0.0 copy-done
  2.2 0.1 constant_dynamic-slice_fusion
  2.3 0.1 copy.23
  2.4 1.3 %reshape.208.gain_ref = bf16[1,2048]{1,0:T(2,128)(2,1)} reshape(bf16[2048]{0:T(1024)(128)(2,1)} %param.26) | data formatting | bytes 8192 | tf_op jit(solution)/shard_map/reshape | solution.py:498
  3.7 0.2 fusion.15
  3.9 0.8 fusion.2
  4.8 0.7 concatenate.19.lat_ref
  5.5 0.1 multiply_cosine_fusion.1
  5.6 0.8 fusion.8
  6.4 0.7 copy.24.qr_ref
  7.1 103.1 %shard_map.167 = (bf16[64,2048]{1,0:T(8,128)(2,1)}, bf16[128,2048]{1,0:T(8,128)(2,1)}) custom-call(bf16[128,2048]{1,0:T(8,128)(2,1)} %x_ref.1, bf16[1,2048]{1,0:T(2,128)(2,1)} %reshape.208.gain_ref, s32[2,128]{1,0:T(2,128)} %bitcast.13, f32[2,128]{1,0:T(2,128)} %bitcast.14, bf16[64,384]{1,0:T(8,128)(2,1)} %concatenate.19.lat_ref, bf16[256,128]{1,0:T(8,128)(2,1)} %q_ref.1, ...), custom_call_target="tpu_custom_call" | custom-call | tf_op jit(solution)/shard_map/pallas_call | solution.py:463
  110.2 1.7 %copy.27 = bf16[64,2048]{1,0:T(8,128)(2,1)} copy(bf16[64,2048]{1,0:T(8,128)(2,1)} %get-tuple-element.10) | data formatting | bytes 524288
  111.9 1.9 %copy.28 = bf16[128,2048]{1,0:T(8,128)(2,1)} copy(bf16[128,2048]{1,0:T(8,128)(2,1)} %get-tuple-element.11) | data formatting | bytes 1048576
  (6 shorter events, 0.0 us)
Async XLA Ops:
  0.6 1.6 %copy-start = (bf16[256,32]{0,1:T(8,128)(2,1)S(1)}, bf16[256,32]{0,1:T(8,128)(2,1)}, u32[]{:S(2)}) copy-start(bf16[256,32]{0,1:T(8,128)(2,1)} %param.19) | copy-start | bytes 49156

commit v2 on v1

--- a/solution.py
+++ b/solution.py
@@ -1,4 +1,5 @@
 import functools
+import math
 import jax
 import jax.numpy as jnp
 from jax import lax
@@ -18,33 +19,13 @@
 BF16 = jnp.bfloat16
 
 
-def normalize(entries, gain):
-    wide = entries.astype(F32)
-    factor = lax.rsqrt(jnp.mean(wide * wide, axis=-1, keepdims=True) + EPSILON)
-    return wide * factor * gain.astype(F32)
-
-
-def rotate(entries, positions):
-    half = entries.shape[-1] // 2
-    freqs = THETA ** (-jnp.arange(half, dtype=F32) / half)
-    angle = positions.astype(F32)[:, None, None] * freqs[None, None, :]
-    cosine = jnp.cos(angle)
-    sine = jnp.sin(angle)
-    first = entries[..., :half].astype(F32)
-    second = entries[..., half:].astype(F32)
-    turned = jnp.concatenate(
-        [first * cosine - second * sine, first * sine + second * cosine], axis=-1
-    )
-    return turned.astype(BF16)
-
-
 def kernel(
     dims,
-    x_ref, gain_ref, routes_ref, weight_ref, lat_ref, q_ref, qr_ref, kw_ref, vw_ref,
+    x_ref, gain_ref, routes_ref, weight_ref, latent_ref, rk_ref, lgain_ref, q_ref, qraw_ref, kw_ref, vw_ref,
     hgain_ref, ow_ref, gate_hbm, up_hbm, down_hbm,
     att_ref, out_ref,
     wgu, wd, outgo, rows, part, hidden, near, pair, across, done, back,
-    lats, total, highest, head_part, head_near, head_pair, head_across,
+    lats, lat_ref, qr_ref, total, highest, head_part, head_near, head_pair, head_across,
     w_sem, z_send, z_recv, fx_send, fx_recv, fc_send, fc_recv, fd_send, fd_recv,
     n_send, n_recv, a_send, a_recv, b_send, b_recv,
     lz_send, lz_recv, lx_send, lx_recv, lc_send, lc_recv, ld_send, ld_recv,
@@ -116,17 +97,55 @@
             lats.at[s, over], lats.at[s, over], ld_send.at[s], ld_recv.at[s], {"tp": mate}
         )
 
+    half = ROTARY_DIM // 2
+
+    def turn(values, repeats, first_position):
+        count, width = values.shape
+        wide_width = width * repeats
+        lane = lax.broadcasted_iota(jnp.int32, (1, wide_width), 1)
+        step = jnp.exp((lane & (half - 1)).astype(F32) * (-math.log(THETA) / half))
+        place = first_position + lax.broadcasted_iota(jnp.int32, (count, 1), 0)
+        angle = place.astype(F32) * step
+        source = lax.broadcasted_iota(jnp.int32, (width, wide_width), 0)
+        target = lax.broadcasted_iota(jnp.int32, (width, wide_width), 1)
+        target = target & (width - 1)
+        low = (target & half) == 0
+        plain = jnp.where(source == target, 1.0, 0.0).astype(BF16)
+        crossed = jnp.where(
+            low & (source == target + half), -1.0,
+            jnp.where((~low) & (source == target - half), 1.0, 0.0),
+        ).astype(BF16)
+        straight = jnp.dot(values, plain, preferred_element_type=F32)
+        other = jnp.dot(values, crossed, preferred_element_type=F32)
+        return (straight * jnp.cos(angle) + other * jnp.sin(angle)).astype(BF16)
+
+    heads = kw_ref.shape[1] // PLAIN_DIM
+    queries = q_ref.shape[0]
+    quarter = lat_ref.shape[0]
+    latent_width = kw_ref.shape[0]
+    rotary_width = heads * ROTARY_DIM
+    scale = (PLAIN_DIM + ROTARY_DIM) ** (-0.5)
+    own_range = pl.ds(pl.multiple_of(t * quarter, quarter), quarter)
+    own_latent = latent_ref[own_range, :].astype(F32)
+    own_factor = lax.rsqrt(jnp.mean(own_latent * own_latent, axis=-1, keepdims=True) + EPSILON)
+    lat_ref[:, :latent_width] = (
+        own_latent * own_factor * lgain_ref[...].astype(F32)[None, :]
+    ).astype(BF16)
+    lat_ref[:, latent_width : latent_width + rotary_width] = turn(
+        rk_ref[own_range, :], heads, e * queries + t * quarter
+    )
+    lats[e, t] = lat_ref[...]
+
     @pl.loop(1, n_ep)
     def _(k):
         lat_z(k, e).start()
 
     lat_x(e, lat_ref).start()
     lat_c(e, lat_ref).start()
-    lats[e, t] = lat_ref[...]
 
     wide = x_ref[...].astype(F32)
     factor = lax.rsqrt(jnp.mean(wide * wide, axis=-1, keepdims=True) + EPSILON)
-    normed = (wide * factor * gain_ref[...].astype(F32)).astype(BF16)
+    normed = (wide * factor * gain_ref[...].astype(F32)[None, :]).astype(BF16)
     before = lax.broadcasted_iota(jnp.int32, (tokens, tokens), 0)
     after = lax.broadcasted_iota(jnp.int32, (tokens, tokens), 1)
     upper = jnp.where(before <= after, 1.0, 0.0).astype(BF16)
@@ -161,23 +180,25 @@
         block = rows.at[s, mine_over, sent]
         return remote(block, block, fd_send.at[s], fd_recv.at[s], {"tp": mate})
 
-    @pl.loop(1, n_ep)
-    def _(k):
+    order = []
+    span = n_ep
+    while span > 1:
+        order += list(range(span // 2, span))
+        span //= 2
+    own_rows = picked_rows(e)
+    rows[e, mine, sent] = own_rows
+    for k in range(1, n_ep):
         outgo[k, sent] = picked_rows(peer(k))
         z_copy(k, e).start()
 
-    rows[e, mine, sent] = picked_rows(e)
+    forward_x(e).start()
+    forward_c(e).start()
+
+    qr_ref[...] = turn(qraw_ref[...], 1, e * queries)
 
     def head_mask(width, h, rows_count):
         lane = lax.broadcasted_iota(jnp.int32, (rows_count, width * heads), 1)
         return (lane >= h * width) & (lane < (h + 1) * width)
-
-    heads = kw_ref.shape[1] // PLAIN_DIM
-    queries = q_ref.shape[0]
-    quarter = lat_ref.shape[0]
-    latent_width = kw_ref.shape[0]
-    rotary_width = heads * ROTARY_DIM
-    scale = (PLAIN_DIM + ROTARY_DIM) ** (-0.5)
 
     def head_c():
         return remote(head_part.at[1 - core], head_near, h_send, h_recv, {"tp": mate})
@@ -242,7 +263,7 @@
             own = jnp.where(inside, total[h], 0.0)
             square = jnp.sum(own * own, axis=-1, keepdims=True) * (1.0 / VALUE_DIM)
             context = context + own * lax.rsqrt(square + EPSILON)
-        head_output = (context * hgain_ref[...].astype(F32)).astype(BF16)
+        head_output = (context * hgain_ref[...].astype(F32)[None, :]).astype(BF16)
         share = jnp.dot(head_output, ow_ref[...], preferred_element_type=F32).astype(BF16)
         for other in range(n_tp):
             head_part[other % 2, other // 2] = share[other * quarter : (other + 1) * quarter]
@@ -287,81 +308,75 @@
             done.at[s, sent], back.at[slot, sent], b_send.at[k], b_recv.at[k], {"ep": s}
         )
 
-    @pl.loop(0, n_ep + 5)
-    def _(it):
-        @pl.when((it >= 2) & (it < n_ep + 2))
-        def _():
-            s = peer(it - 2)
-            forward_c(s).wait_recv()
-            forward_d(s).wait_recv()
-
-            @pl.when(it == 2)
-            def _():
-                for n in range(tiles):
-                    for copy in tile_copies(n):
-                        copy.wait()
-                down_copy.wait()
-
-            multiply(s)
-            near_copy(s).start()
-
-        @pl.when((it >= 3) & (it < n_ep + 3))
-        def _():
-            s = peer(it - 3)
-            near_copy(s).wait_recv()
-            pair[s, sent] = (
-                part[s, core, 1 - side, sent].astype(F32) + near[s, 1 - side, sent].astype(F32)
-            ).astype(BF16)
-            across_copy(s).start()
-
-        @pl.when(it == 2)
-        def _():
-            head_c().wait_recv()
-            head_pair[...] = (
-                head_part[core, 1 - side].astype(F32) + head_near[1 - side].astype(F32)
-            ).astype(BF16)
-            head_x().start()
-
-        @pl.when((it >= 1) & (it < n_ep + 1))
-        def _():
-            s = peer(it - 1)
-            forward_x(s).wait_recv()
-            forward_d(s).start()
-
-        @pl.when((it >= 4) & (it < n_ep + 4))
-        def _():
-            k = it - 4
-            s = peer(k)
-            across_copy(s).wait_recv()
-            final = (
-                part[s, core, side, sent].astype(F32)
-                + near[s, side, sent].astype(F32)
-                + across[s, sent].astype(F32)
-            ).astype(BF16)
-
-            @pl.when(k == 0)
-            def _():
-                back[e, sent] = final
-
-            @pl.when(k > 0)
-            def _():
-                done[s, sent] = final
-                back_copy(k, e).start()
-
-        @pl.when(it < n_ep)
-        def _():
-            s = peer(it)
-
-            @pl.when(it > 0)
-            def _():
-                z_copy(it, s).wait_recv()
-
-            forward_x(s).start()
-            forward_c(s).start()
-
-        @pl.when(it == 0)
-        def _():
-            attend()
+    def arrive(k):
+        s = peer(k)
+        z_copy(k, s).wait_recv()
+        forward_x(s).start()
+        forward_c(s).start()
+
+    def relay(k):
+        s = peer(k)
+        forward_x(s).wait_recv()
+        forward_d(s).start()
+
+    def expert(k):
+        s = peer(k)
+        forward_c(s).wait_recv()
+        forward_d(s).wait_recv()
+        multiply(s)
+        near_copy(s).start()
+
+    def add_near(k):
+        s = peer(k)
+        near_copy(s).wait_recv()
+        pair[s, sent] = (
+            part[s, core, 1 - side, sent].astype(F32) + near[s, 1 - side, sent].astype(F32)
+        ).astype(BF16)
+        across_copy(s).start()
+
+    def finish(k):
+        s = peer(k)
+        across_copy(s).wait_recv()
+        final = (
+            part[s, core, side, sent].astype(F32)
+            + near[s, side, sent].astype(F32)
+            + across[s, sent].astype(F32)
+        ).astype(BF16)
+        if k == 0:
+            back[e, sent] = final
+        else:
+            done[s, sent] = final
+            back_copy(k, e).start()
+
+    attend()
+    relay(0)
+    for n in range(tiles):
+        for copy in tile_copies(n):
+            copy.wait()
+    down_copy.wait()
+    head_c().wait_recv()
+    head_pair[...] = (
+        head_part[core, 1 - side].astype(F32) + head_near[1 - side].astype(F32)
+    ).astype(BF16)
+    head_x().start()
+    expert(0)
+    arrive(order[0])
+    add_near(0)
+    relay(order[0])
+    expert(order[0])
+    for i in range(1, len(order)):
+        last = i == len(order) - 1
+        if not last or i == 0:
+            arrive(order[i])
+        add_near(order[i - 1])
+        if i == len(order) - 2:
+            arrive(order[i + 1])
+        relay(order[i])
+        expert(order[i])
+        finish(order[i - 1])
+    add_near(order[-1])
+    finish(order[-1])
+    finish(0)
 
     head_x().wait_recv()
     att_ref[...] = (
@@ -372,9 +387,7 @@
 
     def gathered(k, acc):
         s = peer(k)
-
-        @pl.when(k > 0)
-        def _():
+        if k > 0:
             back_copy(k, s).wait_recv()
 
         scaled = jnp.where(routes_ref[0:1, :] == s, weight_ref[0:1, :], 0.0)
@@ -390,10 +403,8 @@
     def combine(acc):
         acc[...] = jnp.zeros_like(acc)
 
-        @pl.loop(0, n_ep)
-        def _(k):
+        for k in [0] + order:
             gathered(k, acc)
-
         out_ref[...] = acc[...].astype(BF16)
 
     pl.run_scoped(combine, pltpu.VMEM((tokens, features), F32))
@@ -438,22 +449,8 @@
     units = gate_weight.shape[2]
     tiles = units // LANES
 
-    own = lax.dynamic_slice_in_dim(latent_input, t * quarter, quarter, 0)
-    own_key = lax.dynamic_slice_in_dim(rotary_key, t * quarter, quarter, 0)
-    own_positions = e * count + t * quarter + jnp.arange(quarter, dtype=jnp.int32)
-    latent = normalize(own, latent_gain).astype(BF16)
-    turned = rotate(own_key.reshape(quarter, 1, ROTARY_DIM), own_positions).reshape(
-        quarter, ROTARY_DIM
-    )
-    width = latent.shape[1] + heads * ROTARY_DIM
+    width = latent_input.shape[1] + heads * ROTARY_DIM
     padded = -(-width // LANES) * LANES
-    packed = jnp.concatenate(
-        [latent] + [turned] * heads + [jnp.zeros((quarter, padded - width), BF16)], axis=1
-    )
-    positions = e * count + jnp.arange(count, dtype=jnp.int32)
-    query_rotated = rotate(query_rotary.reshape(count, heads, ROTARY_DIM), positions).reshape(
-        count, heads * ROTARY_DIM
-    )
 
     dma = pltpu.SemaphoreType.DMA
     vmem = pl.BlockSpec(memory_space=pltpu.VMEM)
@@ -466,7 +463,7 @@
             jax.ShapeDtypeStruct((quarter, features), BF16),
             jax.ShapeDtypeStruct((tokens, features), BF16),
         ),
-        in_specs=[vmem] * 11 + [far] * 3,
+        in_specs=[vmem] * 13 + [far] * 3,
         out_specs=(vmem, vmem),
         scratch_shapes=[
             pltpu.VMEM((tiles, features, 2 * LANES), BF16),
@@ -481,6 +478,8 @@
             pltpu.VMEM((n_ep,) + block, BF16),
             pltpu.VMEM((n_ep,) + block, BF16),
             pltpu.VMEM((n_ep, n_tp, quarter, padded), BF16),
+            pltpu.VMEM((quarter, padded), BF16),
+            pltpu.VMEM((count, heads * ROTARY_DIM), BF16),
             pltpu.VMEM((heads, count, heads * VALUE_DIM), F32),
             pltpu.VMEM((heads, count, LANES), F32),
             pltpu.VMEM((2, outer, quarter, features), BF16),
@@ -495,8 +494,8 @@
             collective_id=0, has_side_effects=True, vmem_limit_bytes=60 * 1024 * 1024
         ),
     )(
-        expert_input, expert_gain.reshape(1, -1), routes.T, route_weight.T, packed,
-        query_plain, query_rotated, key_weight, value_weight, head_gain.reshape(1, -1),
+        expert_input, expert_gain, routes.T, route_weight.T, latent_input, rotary_key,
+        latent_gain, query_plain, query_rotary, key_weight, value_weight, head_gain,
         out_weight, gate_weight, up_weight, down_weight,
     )
     return (attended, expert_out)

time: 114 us -> 104 us (0.912)
  the two profiles are of different devices: /device:TPU:9 before, /device:TPU:0 now
where the time goes in v2:
time: 104 us; the launch traced here: 103 us
  Pallas kernels  96.3 us (93%)
  local copies, waits for them, and re-layouts  6.49 us (6%)
    pallas_call x1, Pallas kernels, body(): pl.pallas_call(functools.partial(kernel, (n_ep, n_tp, cap)), out_shape=(j...  96.3 us
    unnamed x4, local copies, waits for them, and re-layouts  6.49 us

profile of v2, /device:TPU:0, one launch (start us, length us, event | category | flops | bytes accessed | tf_op | source)
XLA Modules:
  0.0 103.4 jit_solution(5882544603594314230)
XLA Ops:
  0.6 1.5 %copy.19.qraw_ref = bf16[256,64]{1,0:T(8,128)(2,1)} copy(bf16[256,64]{0,1:T(8,128)(2,1)} %param.17) | data formatting | bytes 65536 | tf_op args[1]
  2.1 1.4 %copy.18.rk_ref = bf16[256,32]{1,0:T(8,128)(2,1)} copy(bf16[256,32]{0,1:T(8,128)(2,1)} %param.19) | data formatting | bytes 32768 | tf_op args[3]
  3.6 96.3 %shard_map.167 = (bf16[64,2048]{1,0:T(8,128)(2,1)}, bf16[128,2048]{1,0:T(8,128)(2,1)}) custom-call(bf16[128,2048]{1,0:T(8,128)(2,1)} %x_ref.1, bf16[2048]{0:T(1024)(128)(2,1)} %gain_ref.1, s32[2,128]{1,0:T(2,128)} %bitcast.2, f32[2,128]{1,0:T(2,128)} %bitcast.3, bf16[256,256]{1,0:T(8,128)(2,1)} %latent_ref.1, bf16[256,32]{1,0:T(8,128)(2,1)} %copy.18.rk_ref, ...), custom_call_target="tpu_custom_call" | custom-call | tf_op jit(solution)/shard_map/pallas_call | solution.py:460
  99.9 1.7 %copy.22 = bf16[64,2048]{1,0:T(8,128)(2,1)} copy(bf16[64,2048]{1,0:T(8,128)(2,1)} %get-tuple-element.4) | data formatting | bytes 524288
  101.6 1.9 %copy.23 = bf16[128,2048]{1,0:T(8,128)(2,1)} copy(bf16[128,2048]{1,0:T(8,128)(2,1)} %get-tuple-element.5) | data formatting | bytes 1048576
